TPU v7x, 32 devices: a whole 2x2x4 slice. The times are simulated.
32 devices in a mesh: sp: 16 (over z, y, core), tp: 2 (over x).
Axes of the slice: x: 2, y: 2, z: 4, core: 2. Of those that a mesh axis runs over, the one named last changes fastest.
Arguments:
- query_rows: bfloat16 [8192, 1024], P(('sp', 'tp')), may hold values from -6 to 6
- key_rows: bfloat16 [8192, 1024], P(('sp', 'tp')), may hold values from -6 to 6
- value_rows: bfloat16 [8192, 1024], P(('sp', 'tp')), may hold values from -6 to 6
- out_grad: bfloat16 [8192, 1024], P(('sp', 'tp')), may hold values from -40 to 40
- log_totals: float32 [8192, 8], P(('sp', 'tp')), may hold values from 6 to 7.5
- out_dot: float32 [8192, 8], P(('sp', 'tp')), may hold values from -6 to 6
- bias_table: float32 [8, 320], replicated, may hold values from -4 to 4
Outputs:
- grad_query: bfloat16 [8192, 1024], P(('sp', 'tp'))
- grad_key: bfloat16 [8192, 1024], P(('sp', 'tp'))
- grad_value: bfloat16 [8192, 1024], P(('sp', 'tp'))
- grad_table: float32 [8, 320], replicated
All inputs are finite; a program needn't handle non-finite values.
Results may differ from a plain program's by a relative error of at most 0.005.
Values may be sent and summed in bfloat16 or wider, within the bound.
No kernel may reach another device: no remote copies, remote signals or barrier semaphores. Data moves between devices by JAX's collectives and lax.ppermute only.
A program may use at most 128 MiB of HBM per device.

v0:
```python
import functools
import math

import jax
import jax.numpy as jnp
from jax import lax
from jax.experimental import pallas as pl
from jax.experimental.pallas import tpu as pltpu
from jax.sharding import PartitionSpec as P


SEG_LEN = 64
AXES = ("sp", "tp")
LOG2E = math.log2(math.e)
MASKED = -1e30
TERMS = 3
ROUND_ORDER = ((0,), (3, 4), (1, 2))
F32 = jnp.float32
BF16 = jnp.bfloat16
NT = (((1,), (1,)), ((), ()))
NN = (((1,), (0,)), ((), ()))


def shifted(block, distance):
    count = lax.axis_size(AXES)
    route = [(i - distance, i) for i in range(count) if 0 <= i - distance < count]
    return lax.ppermute(block, AXES, route)


def pair_tree(parts):
    while len(parts) > 1:
        parts = [parts[i] + parts[i + 1] for i in range(0, len(parts), 2)]
    return parts[0]


def table_rounds(count):
    twos = []
    stride = 1
    while count % (2 * stride) == 0:
        twos.append(stride)
        stride *= 2
    order = ROUND_ORDER
    rounds = [tuple(twos[d] for d in digits if d < len(twos)) for digits in order]
    used = sum(len(digits) for digits in order)
    rounds += [(twos[d],) for d in range(used, len(twos))]
    odd = []
    rest, factor = count // stride, 3
    while rest > 1:
        while rest % factor == 0:
            odd.append((stride, factor))
            stride *= factor
            rest //= factor
        factor += 2
    return [r for r in rounds if r], odd


def all_sum(part):
    count = lax.axis_size(AXES)
    me = lax.axis_index(AXES)
    binary, odd = table_rounds(count)
    for strides in binary:
        masks = [0]
        for stride in strides:
            masks += [mask ^ stride for mask in masks]
        parts = [part]
        for mask in masks[1:]:
            parts.append(lax.ppermute(part, AXES, [(i, i ^ mask) for i in range(count)]))
        part = pair_tree(parts)
    for stride, radix in odd:
        digit = (me // stride) % radix
        parts = [part]
        for step in range(1, radix):
            route = []
            for i in range(count):
                d = (i // stride) % radix
                route.append((i, i + (((d - step) % radix) - d) * stride))
            parts.append(lax.ppermute(part, AXES, route))
        total = jnp.zeros_like(part)
        for d in range(radix):
            value = parts[0]
            for step in range(1, radix):
                value = jnp.where((digit + step) % radix == d, parts[step], value)
            total = total + value
        part = total
    return part


def prep_tiles(head_count, table_ref, chunk_ref, tile_ref):
    size = tile_ref.shape[2]
    table_len = table_ref.shape[1]
    span = chunk_ref.shape[1]
    pad = size - (SEG_LEN - 1)
    lane = lax.broadcasted_iota(jnp.int32, (head_count, span), 1)
    table = table_ref[...] * LOG2E
    first, last = table[:, :1], table[:, table_len - 1 :]
    wide = jnp.concatenate([table, jnp.zeros((head_count, span - table_len), F32)], axis=1)
    moved = pltpu.roll(wide, pad, 1)
    moved = jnp.where(lane < pad, first, jnp.where(lane >= pad + table_len, last, moved))
    chunk_ref[...] = moved
    row = lax.broadcasted_iota(jnp.int32, (size, size), 0)
    col = lax.broadcasted_iota(jnp.int32, (size, size), 1)

    @pl.loop(0, head_count)
    def _(head):
        rolled = []
        lines = chunk_ref[pl.ds(head, 1), :]
        for c in range(4):
            line = jnp.broadcast_to(lines[:, c * size : (c + 1) * size], (size, size))
            rolled.append(pltpu.roll(line, 0, 1, stride=1, stride_axis=0))
        for b in range(3):
            tile = jnp.where(col >= row, rolled[b + 1], rolled[b])
            if b == 0:
                tile = jnp.where((row // SEG_LEN) <= (col // SEG_LEN), tile, MASKED)
            tile_ref[head, b] = tile


def unroll_sum(tile):
    size = tile.shape[0]
    group = 8
    parts = []
    for start in range(0, size, group):
        part = tile[start : start + group, :]
        parts.append(part if start == 0 else pltpu.roll(part, size - start, 1))
    total = pair_tree(parts)
    row = lax.broadcasted_iota(jnp.int32, total.shape, 0)
    for bit in (1, 2, 4):
        total = jnp.where((row & bit) != 0, pltpu.roll(total, size - bit, 1), total)
    return jnp.sum(total, axis=0, keepdims=True)


def score_terms(lag, raw_ref, wgt_ref, w_ref, s_ref, log_row, dot_row, tiles, const, inv_root):
    half = raw_ref.shape[0] // 2
    row = lax.broadcasted_iota(jnp.int32, (half, half), 0) // SEG_LEN
    col = lax.broadcasted_iota(jnp.int32, (half, half), 1) // SEG_LEN
    acc = [None, None, None, None]
    for r in range(2):
        for c in range(2):
            rs, cs = slice(r * half, (r + 1) * half), slice(c * half, (c + 1) * half)
            if (lag == 0 and r > c) or (lag == 2 and c > r):
                w_ref[rs, cs] = jnp.zeros((half, half), BF16)
                s_ref[rs, cs] = jnp.zeros((half, half), BF16)
                continue
            level = min(2 * lag + c - r, 3)
            lrow = log_row[:, cs]
            bias = const - lrow if level == 3 else tiles[level] - lrow
            weight = jnp.exp2(raw_ref[rs, cs] * (inv_root * LOG2E) + bias)
            if lag == 2 and r == c:
                weight = jnp.where(col <= row, weight, 0.0)
            score = weight * (wgt_ref[rs, cs] - dot_row[:, cs])
            acc[level] = score if acc[level] is None else acc[level] + score
            w_ref[rs, cs] = weight.astype(BF16)
            s_ref[rs, cs] = score.astype(BF16)
    return acc


def table_lines(acc, size):
    row = lax.broadcasted_iota(jnp.int32, (size, size), 0)
    col = lax.broadcasted_iota(jnp.int32, (size, size), 1)
    zero = jnp.zeros((size, size), F32)
    lines = []
    for c in range(4):
        upper = acc[c - 1] if c > 0 else None
        lower = acc[c] if c < 3 else None
        line = None
        if upper is not None or lower is not None:
            mixed = jnp.where(
                col >= row,
                zero if upper is None else upper,
                zero if lower is None else lower,
            )
            line = unroll_sum(mixed)
        if c == 3 and acc[3] is not None:
            extra = jnp.sum(acc[3], axis=0, keepdims=True)
            line = extra if line is None else line + extra
        lines.append(line)
    return lines


def fold_table(lines, table_len, size):
    pad = size - (SEG_LEN - 1)
    lane = lax.broadcasted_iota(jnp.int32, lines.shape, 1)
    tail = jnp.sum(jnp.where(lane >= pad + table_len - 1, lines, 0.0), axis=1, keepdims=True)
    moved = pltpu.roll(lines, lines.shape[1] - pad, 1)[:, :table_len]
    lane = lax.broadcasted_iota(jnp.int32, moved.shape, 1)
    return jnp.where(lane == table_len - 1, tail, moved)


def pack_height(count, rows, width):
    lines = -(-count * TERMS * rows // width)
    return -(-lines // 8) * 8


def pack_lines(stats, width):
    count, rows = stats.shape
    high = stats.astype(BF16).astype(F32)
    rest = stats - high
    mid = rest.astype(BF16).astype(F32)
    terms = (high, mid, rest - mid)
    per_row = width // rows
    lines = []
    for line in range(pack_height(count, rows, width)):
        pieces = []
        for b in range(line * per_row, (line + 1) * per_row):
            if b < count * TERMS:
                pieces.append(terms[b // count][b % count : b % count + 1, :])
            else:
                pieces.append(jnp.zeros((1, rows), F32))
        lines.append(jnp.concatenate(pieces, axis=1))
    return jnp.concatenate(lines, axis=0).astype(BF16)


def unpack_lines(pack_ref, stat_ref):
    count, rows = stat_ref.shape
    per_row = pack_ref.shape[1] // rows
    packed = pack_ref[rows:, :].astype(F32)
    for i in range(count):
        total = None
        for term in range(TERMS):
            line, at = divmod(term * count + i, per_row)
            piece = packed[line : line + 1, at * rows : (at + 1) * rows]
            total = piece if total is None else total + piece
        stat_ref[i : i + 1, :] = total


def prep_kernel(g_hbm, log_hbm, dot_hbm, far_ref, first_ref, second_ref, stat_ref,
                log_ref, dot_ref, sems):
    rows, feats = g_hbm.shape
    cut = first_ref.shape[1]
    moves = (
        (log_hbm, log_ref),
        (dot_hbm, dot_ref),
        (g_hbm, far_ref.at[pl.ds(0, rows), :]),
        (g_hbm.at[:, pl.ds(0, cut)], first_ref.at[pl.ds(0, rows), :]),
        (g_hbm.at[:, pl.ds(cut, feats - cut)], second_ref),
    )
    copies = []
    for i, (origin, target) in enumerate(moves):
        copies.append(pltpu.make_async_copy(origin, target, sems.at[i]))
        copies[-1].start()
    for copy in copies[:2]:
        copy.wait()
    stats = jnp.concatenate([log_ref[...] * LOG2E, dot_ref[...]], axis=0)
    stat_ref[...] = stats
    first_ref[rows:, :] = pack_lines(stats, first_ref.shape[1])
    far_ref[rows:, :] = pack_lines(stats, far_ref.shape[1])
    for copy in copies[2:]:
        copy.wait()


def lag_kernel(lag, first_head, last_head, head_count, *refs):
    raw_refs, wgt_refs, w_refs, s_refs = (refs[len(refs) - 8 + 2 * i :][:2] for i in range(4))
    refs = refs[:-8]
    if lag == 0:
        (k_hbm, v_hbm, q_hbm, table_hbm, g_ref, stat_ref,
         dq_ref, dk_ref, dv_ref, tab_ref, kt_ref, tile_ref, chunk_ref, k_ref, v_ref,
         q_ref, table_ref, sems) = refs
        pairs = ((table_hbm, table_ref), (k_hbm, k_ref), (v_hbm, v_ref), (q_hbm, q_ref))
        copies = []
        for i, (source, target) in enumerate(pairs):
            copies.append(pltpu.make_async_copy(source, target, sems.at[i]))
            copies[-1].start()
        copies[0].wait()
        prep_tiles(head_count, table_ref, chunk_ref, tile_ref)
        for copy in copies[1:]:
            copy.wait()
    elif lag == 2:
        (k_ref, v_ref, kt_ref, tile_ref, chunk_ref, dk_in, dv_in, tab_in, q_ref, g_ref,
         dk_ref, dv_ref, tab_ref, dq_ref, stat_ref) = refs
        unpack_lines(g_ref, stat_ref)
    elif first_head == 0:
        (k_ref, v_ref, kt_ref, tile_ref, chunk_ref, dk_in, dv_in, tab_in, q_ref, g_ref,
         dk_ref, dv_ref, tab_ref, dq_ref, stat_ref) = refs
        unpack_lines(g_ref, stat_ref)
    else:
        (k_ref, v_ref, kt_ref, tile_ref, chunk_ref, dk_in, dv_in, tab_in, q_ref, g_ref,
         stat_ref, _, dk_ref, dv_ref, out_tab_ref, dq_ref) = refs
    rows = k_ref.shape[0]
    size = tile_ref.shape[2]
    head_dim = k_ref.shape[1] // head_count
    inv_root = head_dim ** (-0.5)
    g_shift = -first_head * head_dim
    last_lines = []

    def span(head):
        return slice(head * head_dim, (head + 1) * head_dim)

    def products(head, at):
        local = slice(head * head_dim + g_shift, (head + 1) * head_dim + g_shift)
        query, grad = q_ref[:, span(head)], g_ref[:rows, local]
        raw_refs[at][...] = lax.dot_general(
            k_ref[:, span(head)], query, NT, preferred_element_type=F32
        )
        wgt_refs[at][...] = lax.dot_general(
            v_ref[:, span(head)], grad, NT, preferred_element_type=F32
        )

    def scores(head, at):
        log_row = stat_ref[head : head + 1, :]
        dot_row = stat_ref[head + head_count : head + head_count + 1, :]
        const = chunk_ref[head : head + 1, 3 * size :]
        tiles = [None if lag == 2 else tile_ref[head, b] for b in range(3)]
        acc = score_terms(
            lag, raw_refs[at], wgt_refs[at], w_refs[at], s_refs[at],
            log_row, dot_row, tiles, const, inv_root,
        )
        lines = [
            jnp.zeros((1, size), F32) if line is None else line for line in table_lines(acc, size)
        ]
        lines = jnp.concatenate(lines, axis=1)
        if lag > 0:
            lines = tab_in[head : head + 1, :] + lines
        if first_head == 0:
            tab_ref[head : head + 1, :] = lines
        else:
            last_lines.append(lines)

    def gradients(head, at):
        cols = span(head)
        local = slice(head * head_dim + g_shift, (head + 1) * head_dim + g_shift)
        if lag == 0:
            turned = k_ref[:, cols].T
            kt_ref[cols, :] = turned
        else:
            turned = kt_ref[cols, :]
        score_b = s_refs[at][...]
        dq = lax.dot_general(turned, score_b, NN, preferred_element_type=F32) * inv_root
        dq_ref[cols, :] = dq.astype(dq_ref.dtype)
        dk = lax.dot_general(score_b, q_ref[:, cols], NN, preferred_element_type=F32)
        dv = lax.dot_general(w_refs[at][...], g_ref[:rows, local], NN, preferred_element_type=F32)
        if lag > 0:
            dk = dk + dk_in[:, cols]
            dv = dv + dv_in[:, cols]
        dk_ref[:, cols] = dk
        dv_ref[:, cols] = dv

    stages = (products, scores, gradients)
    steps = last_head - first_head + len(stages) - 1
    for step in range(steps):
        for depth, stage in enumerate(stages):
            head = first_head + step - depth
            if first_head <= head < last_head:
                stage(head, head % 2)

    if first_head > 0:
        table = jnp.concatenate([tab_in[:first_head, :]] + last_lines, axis=0)
        out_tab_ref[...] = fold_table(table, out_tab_ref.shape[1], size)


def key_value_kernel(scale, dk_ref, dv_ref, gk_hbm, gv_hbm, gk_ref, gv_ref, sems):
    gk_ref[...] = (dk_ref[...] * scale).astype(BF16)
    copies = [pltpu.make_async_copy(gk_ref, gk_hbm, sems.at[0])]
    copies[0].start()
    gv_ref[...] = dv_ref[...].astype(BF16)
    copies.append(pltpu.make_async_copy(gv_ref, gv_hbm, sems.at[1]))
    copies[1].start()
    for copy in copies:
        copy.wait()


def query_kernel(head_count, dq_ref, one_ref, two_ref, gq_hbm, gq_ref, sems):
    head_dim = dq_ref.shape[0] // head_count
    copies = []
    for head in range(head_count):
        cols = slice(head * head_dim, (head + 1) * head_dim)
        total = dq_ref[cols, :] + one_ref[cols, :].astype(F32) + two_ref[cols, :].astype(F32)
        gq_ref[:, cols] = total.T.astype(BF16)
        if head % 4 == 3:
            part = pl.ds((head - 3) * head_dim, 4 * head_dim)
            copies.append(
                pltpu.make_async_copy(gq_ref.at[:, part], gq_hbm.at[:, part], sems.at[head // 4])
            )
            copies[-1].start()
    for copy in copies:
        copy.wait()


def local(query_rows, key_rows, value_rows, out_grad, log_totals, out_dot, bias_table):
    rows, feats = query_rows.shape
    heads = log_totals.shape[1]
    table_len = bias_table.shape[1]
    half = rows // 2
    cut_head = heads * 3 // 4
    head_dim = feats // heads
    cut = cut_head * head_dim
    vmem = pl.BlockSpec(memory_space=pltpu.VMEM)
    hbm = pl.BlockSpec(memory_space=pltpu.HBM)
    pair_flops = 2 * rows * rows * head_dim

    def call(body, work, outs, args, scratch=(), specs=None, out_specs=None, aliases={}):
        estimate = pl.CostEstimate(
            flops=int(work * pair_flops), bytes_accessed=8 * rows * feats, transcendentals=0
        )
        return pl.pallas_call(
            body,
            in_specs=[vmem] * len(args) if specs is None else specs,
            out_specs=[vmem] * len(outs) if out_specs is None else out_specs,
            out_shape=outs,
            scratch_shapes=list(scratch),
            input_output_aliases=aliases,
            cost_estimate=estimate,
            compiler_params=pltpu.CompilerParams(vmem_limit_bytes=16 * 2**20),
        )(*args)

    rows_f32 = pltpu.VMEM((rows, feats), F32)
    rows_b16 = pltpu.VMEM((rows, feats), BF16)
    turn_f32 = pltpu.VMEM((feats, rows), F32)
    turn_b16 = pltpu.VMEM((feats, rows), BF16)
    wide_tab = pltpu.VMEM((heads, 4 * half), F32)
    table_shape = pltpu.VMEM((heads, table_len), F32)
    tile_shape = pltpu.VMEM((heads, 3, half, half), F32)
    stat_shape = pltpu.VMEM((2 * heads, rows), F32)
    line_shape = pltpu.VMEM((heads, rows), F32)
    out_shape = jax.ShapeDtypeStruct((rows, feats), BF16)
    stage_shapes = (pltpu.VMEM((rows, rows), F32),) * 4 + (pltpu.VMEM((rows, rows), BF16),) * 4
    body = functools.partial

    def at_hbm(array):
        return pltpu.with_memory_space_constraint(array, pltpu.HBM)

    def packed_shape(height, width):
        return pltpu.VMEM((height + pack_height(2 * heads, rows, width), width), BF16)

    query_far = shifted(query_rows, -2)
    query_in = shifted(query_rows, -1)
    far, first, second, stats = call(
        prep_kernel, 1,
        [packed_shape(rows, feats), packed_shape(rows, cut),
         pltpu.VMEM((rows, feats - cut), BF16), stat_shape],
        tuple(at_hbm(x) for x in (out_grad, log_totals.T, out_dot.T)),
        (line_shape, line_shape, pltpu.SemaphoreType.DMA((5,))),
        [hbm] * 3,
    )
    far_in = shifted(far, -2)
    first_in = shifted(first, -1)
    second_in = shifted(second, -1)

    dq0, dk, dv, tab, turned, tiles, chunks, keys, values = call(
        body(lag_kernel, 0, 0, heads, heads), 5 * heads,
        [turn_f32, rows_f32, rows_f32, wide_tab, turn_b16, tile_shape, wide_tab,
         rows_b16, rows_b16],
        tuple(at_hbm(x) for x in (key_rows, value_rows, query_rows, bias_table))
        + (far, stats),
        (rows_b16, table_shape, pltpu.SemaphoreType.DMA((4,))) + stage_shapes,
        [hbm] * 4 + [vmem] * 2,
    )
    shared = (keys, values, turned, tiles, chunks)
    dk, dv, tab, dq2, _ = call(
        body(lag_kernel, 2, 0, heads, heads), 5 * heads,
        [rows_f32, rows_f32, wide_tab, turn_b16, stat_shape],
        shared + (dk, dv, tab, query_far, far_in), stage_shapes, aliases={5: 0, 6: 1, 7: 2},
    )
    back_far = shifted(dq2, 2)
    dk, dv, tab, dq1, stats_in = call(
        body(lag_kernel, 1, 0, cut_head, heads), 5 * cut_head,
        [rows_f32, rows_f32, wide_tab, turn_b16, stat_shape],
        shared + (dk, dv, tab) + (query_in, first_in), stage_shapes, aliases={5: 0, 6: 1, 7: 2},
    )
    dk, dv, table_part, dq1 = call(
        body(lag_kernel, 1, cut_head, heads, heads), 5 * (heads - cut_head),
        [rows_f32, rows_f32, table_shape, turn_b16],
        shared + (dk, dv, tab) + (query_in, second_in, stats_in, dq1), stage_shapes,
        aliases={5: 0, 6: 1, 11: 3},
    )
    back_near = shifted(dq1, 1)
    grad_table = all_sum(table_part)
    grad_key, grad_value = call(
        body(key_value_kernel, head_dim ** (-0.5)), 1, [out_shape] * 2, (dk, dv),
        (rows_b16,) * 2 + (pltpu.SemaphoreType.DMA((2,)),), out_specs=[hbm] * 2,
    )
    grad_query, = call(
        body(query_kernel, heads), 1, [out_shape], (dq0, back_near, back_far),
        (rows_b16, pltpu.SemaphoreType.DMA((heads // 4,))), out_specs=[hbm],
    )
    return grad_query, grad_key, grad_value, grad_table


def solution(mesh):
    placed = (P(AXES, None),) * 6 + (P(),)
    return jax.shard_map(
        local,
        mesh=mesh,
        in_specs=placed,
        out_specs=(P(AXES, None),) * 3 + (P(),),
        check_vma=False,
    )
```

profile of v0, /device:TPU:0, one launch (start us, length us, event | category | flops | bytes accessed | tf_op | source)
XLA Modules:
  0.0 67.0 jit_solution(4962708443400629002)
XLA Ops:
  0.6 1.3 %shard_map.102 = (bf16[272,1024]{1,0:T(8,128)(2,1)S(1)}, bf16[272,768]{1,0:T(8,128)(2,1)S(1)}, bf16[256,256]{1,0:T(8,128)(2,1)S(1)}, f32[16,256]{1,0:T(8,128)S(1)}) custom-call(bf16[256,1024]{1,0:T(8,128)(2,1)} %g_hbm.1, f32[8,256]{1,0:T(8,128)} %bitcast.2, f32[8,256]{1,0:T(8,128)} %bitcast.3), custom_call_target="tpu_custom_call" | custom-call | flops 16777216 | bytes 2097152 | tf_op jit(solution)/shard_map/pallas_call | solution.py:393
  1.9 1.3 %collective-permute-start.1 = (bf16[272,1024]{1,0:T(8,128)(2,1)S(1)}, bf16[272,1024]{1,0:T(8,128)(2,1)S(1)}, u32[]{:S(2)}, u32[]{:S(2)}) collective-permute-start(bf16[272,1024]{1,0:T(8,128)(2,1)S(1)} %get-tuple-element.32.refs_4_), channel_id=1, source_target_pairs={{2,0},{3,1},{4,2},{5,3},{6,4},{7,5},{8,6},{9,7},{10,8},{11,9},{12,... | collective-permute-start | bytes 1671176 | tf_op jit(solution)/shard_map/ppermute | solution.py:27
  3.2 1.3 %collective-permute-start = (bf16[256,1024]{1,0:T(8,128)(2,1)}, bf16[256,1024]{1,0:T(8,128)(2,1)S(1)}, u32[]{:S(2)}, u32[]{:S(2)}) collective-permute-start(bf16[256,1024]{1,0:T(8,128)(2,1)} %refs_2_.1), channel_id=1, source_target_pairs={{2,0},{3,1},{4,2},{5,3},{6,4},{7,5},{8,6},{9,7},{10,8},{11,9},{12,... | collective-permute-start | bytes 1572872 | tf_op jit(solution)/shard_map/ppermute | solution.py:27
  4.5 1.3 %collective-permute-start.2 = (bf16[256,1024]{1,0:T(8,128)(2,1)}, bf16[256,1024]{1,0:T(8,128)(2,1)S(1)}, u32[]{:S(2)}, u32[]{:S(2)}) collective-permute-start(bf16[256,1024]{1,0:T(8,128)(2,1)} %refs_2_.1), channel_id=1, source_target_pairs={{1,0},{2,1},{3,2},{4,3},{5,4},{6,5},{7,6},{8,7},{9,8},{10,9},{11,1... | collective-permute-start | bytes 1572872 | tf_op jit(solution)/shard_map/ppermute | solution.py:27
  5.8 1.3 %collective-permute-start.3 = (bf16[272,768]{1,0:T(8,128)(2,1)S(1)}, bf16[272,768]{1,0:T(8,128)(2,1)S(1)}, u32[]{:S(2)}, u32[]{:S(2)}) collective-permute-start(bf16[272,768]{1,0:T(8,128)(2,1)S(1)} %get-tuple-element.46), channel_id=1, source_target_pairs={{1,0},{2,1},{3,2},{4,3},{5,4},{6,5},{7,6},{8,7},{9,8},{10,9},{11,1... | collective-permute-start | bytes 1253384 | tf_op jit(solution)/shard_map/ppermute | solution.py:27
  7.1 1.3 %collective-permute-start.4 = (bf16[256,256]{1,0:T(8,128)(2,1)S(1)}, bf16[256,256]{1,0:T(8,128)(2,1)S(1)}, u32[]{:S(2)}, u32[]{:S(2)}) collective-permute-start(bf16[256,256]{1,0:T(8,128)(2,1)S(1)} %get-tuple-element.50), channel_id=1, source_target_pairs={{1,0},{2,1},{3,2},{4,3},{5,4},{6,5},{7,6},{8,7},{9,8},{10,9},{11,1... | collective-permute-start | bytes 393224 | tf_op jit(solution)/shard_map/ppermute | solution.py:27
  8.4 3.6 %shard_map.103 = (f32[1024,256]{1,0:T(8,128)S(1)}, f32[256,1024]{1,0:T(8,128)S(1)}, f32[256,1024]{1,0:T(8,128)S(1)}, f32[8,512]{1,0:T(8,128)S(1)}, bf16[1024,256...) custom-call(bf16[256,1024]{1,0:T(8,128)(2,1)} %refs_0_.1, ...), custom_call_target="tpu_custom_call" | custom-call | flops 671088640 | bytes 2097152 | tf_op jit(solution)/shard_map/pallas_call | solution.py:393
  12.0 0.0 collective-permute-done.refs_8_
  12.0 0.0 collective-permute-done.1.refs_9_
  12.1 2.1 %shard_map.104 = (f32[256,1024]{1,0:T(8,128)S(1)}, f32[256,1024]{1,0:T(8,128)S(1)}, f32[8,512]{1,0:T(8,128)S(1)}, bf16[1024,256]{1,0:T(8,128)(2,1)S(1)}, f32[16,256]{1,0:T(8,128)}) custom-call(bf16[256,1024]{1,0:T(8,128)(2,1)S(1)} %get-tuple-element.35.refs_0_, ...), custom_call_target="tpu_custom_call", output_to_operand_aliasing={{0}: (5, {}), {1}: (6, {}), {2}: (7, {})} | custom-call | flops 671088640 | bytes 2097152 | tf_op jit(solution)/shard_map/pallas_call | solution.py:393
  14.2 16.1 %collective-permute-done.3.refs_9_ = bf16[272,768]{1,0:T(8,128)(2,1)S(1)} collective-permute-done((bf16[272,768]{1,0:T(8,128)(2,1)S(1)}, bf16[272,768]{1,0:T(8,128)(2,1)S(1)}, u32[]{:S(2)}, u32[]{:S(2)}) %collective-permute-start.3) | collective-permute-done | bytes 417824 | tf_op jit(solution)/shard_map/ppermute | solution.py:27
  30.2 0.0 collective-permute-done.2.refs_8_
  30.2 1.5 %shard_map.105 = (f32[256,1024]{1,0:T(8,128)S(1)}, f32[256,1024]{1,0:T(8,128)S(1)}, f32[8,512]{1,0:T(8,128)S(1)}, bf16[1024,256]{1,0:T(8,128)(2,1)S(1)}, f32[16,256]{1,0:T(8,128)S(1)}) custom-call(bf16[256,1024]{1,0:T(8,128)(2,1)S(1)} %get-tuple-element.35.refs_0_, ...), custom_call_target="tpu_custom_call", output_to_operand_aliasing={{0}: (5, {}), {1}: (6, {}), {2}: (7, {})} | custom-call | flops 503316480 | bytes 2097152 | tf_op jit(solution)/shard_map/pallas_call | solution.py:393
  31.7 1.3 %collective-permute-done.4.refs_9_ = bf16[256,256]{1,0:T(8,128)(2,1)S(1)} collective-permute-done((bf16[256,256]{1,0:T(8,128)(2,1)S(1)}, bf16[256,256]{1,0:T(8,128)(2,1)S(1)}, u32[]{:S(2)}, u32[]{:S(2)}) %collective-permute-start.4) | collective-permute-done | bytes 131104 | tf_op jit(solution)/shard_map/ppermute | solution.py:27
  33.0 0.8 %shard_map.106 = (f32[256,1024]{1,0:T(8,128)S(1)}, f32[256,1024]{1,0:T(8,128)S(1)}, f32[8,320]{1,0:T(8,128)S(1)}, bf16[1024,256]{1,0:T(8,128)(2,1)S(1)}) custom-call(bf16[256,1024]{1,0:T(8,128)(2,1)S(1)} %get-tuple-element.35.refs_0_, bf16[256,1024]{1,0:T(8,128)(2,1)S(1)} %get-tuple-element.36.refs_1_, ...), custom_call_target="tpu_custom_call", output_to_operand_aliasing={{0}: (5, {}), {1}: (6, {}), {3}: (11, {})} | custom-call | flops 167772160 | bytes 2097152 | tf_op jit(solution)/shard_map/pallas_call | solution.py:393
  33.8 4.6 %collective-permute-start.5 = (bf16[1024,256]{1,0:T(8,128)(2,1)S(1)}, bf16[1024,256]{1,0:T(8,128)(2,1)S(1)}, u32[]{:S(2)}, u32[]{:S(2)}) collective-permute-start(bf16[1024,256]{1,0:T(8,128)(2,1)S(1)} %get-tuple-element.53), channel_id=1, source_target_pairs={{0,1},{1,2},{2,3},{3,4},{4,5},{5,6},{6,7},{7,8},{8,9},{9,10},{10,1... | collective-permute-start | bytes 1572872 | tf_op jit(solution)/shard_map/ppermute | solution.py:27
  38.4 4.2 %collective-permute-start.6 = (bf16[1024,256]{1,0:T(8,128)(2,1)S(1)}, bf16[1024,256]{1,0:T(8,128)(2,1)S(1)}, u32[]{:S(2)}, u32[]{:S(2)}) collective-permute-start(bf16[1024,256]{1,0:T(8,128)(2,1)S(1)} %get-tuple-element.54), channel_id=1, source_target_pairs={{0,2},{1,3},{2,4},{3,5},{4,6},{5,7},{6,8},{7,9},{8,10},{9,11},{10,... | collective-permute-start | bytes 1572872 | tf_op jit(solution)/shard_map/ppermute | solution.py:27
  42.6 0.7 %collective-permute-start.7 = (f32[8,320]{1,0:T(8,128)S(1)}, f32[8,320]{1,0:T(8,128)S(1)}, u32[]{:S(2)}, u32[]{:S(2)}) collective-permute-start(f32[8,320]{1,0:T(8,128)S(1)} %get-tuple-element.59), channel_id=1, source_target_pairs={{0,1},{1,0},{2,3},{3,2},{4,5},{5,4},{6,7},{7,6},{8,9},{9,8},{10,11... | collective-permute-start | bytes 30728 | tf_op jit(solution)/shard_map/ppermute | solution.py:67
  43.2 6.1 %collective-permute-done.7 = f32[8,320]{1,0:T(8,128)S(1)} collective-permute-done((f32[8,320]{1,0:T(8,128)S(1)}, f32[8,320]{1,0:T(8,128)S(1)}, u32[]{:S(2)}, u32[]{:S(2)}) %collective-permute-start.7) | collective-permute-done | bytes 10272 | tf_op jit(solution)/shard_map/ppermute | solution.py:67
  49.4 6.8 %collective-permute-start.9 = (f32[8,320]{1,0:T(8,128)S(1)}, f32[8,320]{1,0:T(8,128)S(1)}, u32[]{:S(2)}, u32[]{:S(2)}) collective-permute-start(f32[8,320]{1,0:T(8,128)S(1)} %add.21), channel_id=1, source_target_pairs={{0,16},{1,17},{2,18},{3,19},{4,20},{5,21},{6,22},{7,23},{8,24},{9,... | collective-permute-start | bytes 30728 | tf_op jit(solution)/shard_map/ppermute | solution.py:67
  56.1 1.3 %collective-permute-start.10 = (f32[8,320]{1,0:T(8,128)S(1)}, f32[8,320]{1,0:T(8,128)S(1)}, u32[]{:S(2)}, u32[]{:S(2)}) collective-permute-start(f32[8,320]{1,0:T(8,128)S(1)} %add.21), channel_id=1, source_target_pairs={{0,24},{1,25},{2,26},{3,27},{4,28},{5,29},{6,30},{7,31},{8,16},{9,... | collective-permute-start | bytes 30728 | tf_op jit(solution)/shard_map/ppermute | solution.py:67
  57.5 0.0 collective-permute-start.8
  57.5 0.3 collective-permute-done.9
  57.8 3.8 %collective-permute-done.10 = f32[8,320]{1,0:T(8,128)S(1)} collective-permute-done((f32[8,320]{1,0:T(8,128)S(1)}, f32[8,320]{1,0:T(8,128)S(1)}, u32[]{:S(2)}, u32[]{:S(2)}) %collective-permute-start.10) | collective-permute-done | bytes 10272 | tf_op jit(solution)/shard_map/ppermute | solution.py:67
  61.6 0.0 collective-permute-done.8
  61.6 0.3 collective-permute-start.12
  62.0 0.0 collective-permute-start.13
  62.0 1.9 %collective-permute-start.11 = (f32[8,320]{1,0:T(8,128)S(1)}, f32[8,320]{1,0:T(8,128)S(1)}, u32[]{:S(2)}, u32[]{:S(2)}) collective-permute-start(f32[8,320]{1,0:T(8,128)S(1)} %add_add_fusion.1), channel_id=1, source_target_pairs={{0,2},{1,3},{2,0},{3,1},{4,6},{5,7},{6,4},{7,5},{8,10},{9,11},{10,... | collective-permute-start | bytes 30728 | tf_op jit(solution)/shard_map/ppermute | solution.py:67
  63.9 1.1 %shard_map.108 = (bf16[256,1024]{1,0:T(8,128)(2,1)}, bf16[256,1024]{1,0:T(8,128)(2,1)}) custom-call(f32[256,1024]{1,0:T(8,128)S(1)} %get-tuple-element.55.dk_ref, f32[256,1024]{1,0:T(8,128)S(1)} %get-tuple-element.56.dv_ref), custom_call_target="tpu_custom_call" | custom-call | flops 16777216 | bytes 2097152 | tf_op jit(solution)/shard_map/pallas_call | solution.py:393
  64.9 0.5 collective-permute-done.12
  65.4 0.6 add_add_fusion
  66.0 1.0 %shard_map.107 = bf16[256,1024]{1,0:T(8,128)(2,1)} custom-call(f32[1024,256]{1,0:T(8,128)S(1)} %get-tuple-element.34.dq_ref, bf16[1024,256]{1,0:T(8,128)(2,1)S(1)} %collective-permute-done.5.one_ref, bf16[1024,256]{1,0:T(8,128)(2,1)S(1)} %collective-permute-done.6.two_ref), custom_call_target="tpu_custom_call" | custom-call | flops 16777216 | bytes 2097152 | tf_op jit(solution)/shard_map/pallas_call | solution.py:393
  (6 shorter events, 0.0 us)
Async XLA Ops:
  1.9 10.2 %collective-permute-start.1 = (bf16[272,1024]{1,0:T(8,128)(2,1)S(1)}, bf16[272,1024]{1,0:T(8,128)(2,1)S(1)}, u32[]{:S(2)}, u32[]{:S(2)}) collective-permute-start(bf16[272,1024]{1,0:T(8,128)(2,1)S(1)} %get-tuple-element.32.refs_4_), channel_id=1, source_target_pairs={{2,0},{3,1},{4,2},{5,3},{6,4},{7,5},{8,6},{9,7},{10,8},{11,9},{12,... | collective-permute-start | bytes 1671176 | tf_op jit(solution)/shard_map/ppermute | solution.py:27
  3.2 8.8 %collective-permute-start = (bf16[256,1024]{1,0:T(8,128)(2,1)}, bf16[256,1024]{1,0:T(8,128)(2,1)S(1)}, u32[]{:S(2)}, u32[]{:S(2)}) collective-permute-start(bf16[256,1024]{1,0:T(8,128)(2,1)} %refs_2_.1), channel_id=1, source_target_pairs={{2,0},{3,1},{4,2},{5,3},{6,4},{7,5},{8,6},{9,7},{10,8},{11,9},{12,... | collective-permute-start | bytes 1572872 | tf_op jit(solution)/shard_map/ppermute | solution.py:27
  4.5 25.7 %collective-permute-start.2 = (bf16[256,1024]{1,0:T(8,128)(2,1)}, bf16[256,1024]{1,0:T(8,128)(2,1)S(1)}, u32[]{:S(2)}, u32[]{:S(2)}) collective-permute-start(bf16[256,1024]{1,0:T(8,128)(2,1)} %refs_2_.1), channel_id=1, source_target_pairs={{1,0},{2,1},{3,2},{4,3},{5,4},{6,5},{7,6},{8,7},{9,8},{10,9},{11,1... | collective-permute-start | bytes 1572872 | tf_op jit(solution)/shard_map/ppermute | solution.py:27
  5.8 24.4 %collective-permute-start.3 = (bf16[272,768]{1,0:T(8,128)(2,1)S(1)}, bf16[272,768]{1,0:T(8,128)(2,1)S(1)}, u32[]{:S(2)}, u32[]{:S(2)}) collective-permute-start(bf16[272,768]{1,0:T(8,128)(2,1)S(1)} %get-tuple-element.46), channel_id=1, source_target_pairs={{1,0},{2,1},{3,2},{4,3},{5,4},{6,5},{7,6},{8,7},{9,8},{10,9},{11,1... | collective-permute-start | bytes 1253384 | tf_op jit(solution)/shard_map/ppermute | solution.py:27
  7.1 26.0 %collective-permute-start.4 = (bf16[256,256]{1,0:T(8,128)(2,1)S(1)}, bf16[256,256]{1,0:T(8,128)(2,1)S(1)}, u32[]{:S(2)}, u32[]{:S(2)}) collective-permute-start(bf16[256,256]{1,0:T(8,128)(2,1)S(1)} %get-tuple-element.50), channel_id=1, source_target_pairs={{1,0},{2,1},{3,2},{4,3},{5,4},{6,5},{7,6},{8,7},{9,8},{10,9},{11,1... | collective-permute-start | bytes 393224 | tf_op jit(solution)/shard_map/ppermute | solution.py:27
  33.8 32.2 %collective-permute-start.5 = (bf16[1024,256]{1,0:T(8,128)(2,1)S(1)}, bf16[1024,256]{1,0:T(8,128)(2,1)S(1)}, u32[]{:S(2)}, u32[]{:S(2)}) collective-permute-start(bf16[1024,256]{1,0:T(8,128)(2,1)S(1)} %get-tuple-element.53), channel_id=1, source_target_pairs={{0,1},{1,2},{2,3},{3,4},{4,5},{5,6},{6,7},{7,8},{8,9},{9,10},{10,1... | collective-permute-start | bytes 1572872 | tf_op jit(solution)/shard_map/ppermute | solution.py:27
  38.4 27.6 %collective-permute-start.6 = (bf16[1024,256]{1,0:T(8,128)(2,1)S(1)}, bf16[1024,256]{1,0:T(8,128)(2,1)S(1)}, u32[]{:S(2)}, u32[]{:S(2)}) collective-permute-start(bf16[1024,256]{1,0:T(8,128)(2,1)S(1)} %get-tuple-element.54), channel_id=1, source_target_pairs={{0,2},{1,3},{2,4},{3,5},{4,6},{5,7},{6,8},{7,9},{8,10},{9,11},{10,... | collective-permute-start | bytes 1572872 | tf_op jit(solution)/shard_map/ppermute | solution.py:27
  42.6 6.8 %collective-permute-start.7 = (f32[8,320]{1,0:T(8,128)S(1)}, f32[8,320]{1,0:T(8,128)S(1)}, u32[]{:S(2)}, u32[]{:S(2)}) collective-permute-start(f32[8,320]{1,0:T(8,128)S(1)} %get-tuple-element.59), channel_id=1, source_target_pairs={{0,1},{1,0},{2,3},{3,2},{4,5},{5,4},{6,7},{7,6},{8,9},{9,8},{10,11... | collective-permute-start | bytes 30728 | tf_op jit(solution)/shard_map/ppermute | solution.py:67
  49.4 8.5 %collective-permute-start.9 = (f32[8,320]{1,0:T(8,128)S(1)}, f32[8,320]{1,0:T(8,128)S(1)}, u32[]{:S(2)}, u32[]{:S(2)}) collective-permute-start(f32[8,320]{1,0:T(8,128)S(1)} %add.21), channel_id=1, source_target_pairs={{0,16},{1,17},{2,18},{3,19},{4,20},{5,21},{6,22},{7,23},{8,24},{9,... | collective-permute-start | bytes 30728 | tf_op jit(solution)/shard_map/ppermute | solution.py:67
  56.1 5.5 %collective-permute-start.10 = (f32[8,320]{1,0:T(8,128)S(1)}, f32[8,320]{1,0:T(8,128)S(1)}, u32[]{:S(2)}, u32[]{:S(2)}) collective-permute-start(f32[8,320]{1,0:T(8,128)S(1)} %add.21), channel_id=1, source_target_pairs={{0,24},{1,25},{2,26},{3,27},{4,28},{5,29},{6,30},{7,31},{8,16},{9,... | collective-permute-start | bytes 30728 | tf_op jit(solution)/shard_map/ppermute | solution.py:67
  57.5 4.1 %collective-permute-start.8 = (f32[8,320]{1,0:T(8,128)S(1)}, f32[8,320]{1,0:T(8,128)S(1)}, u32[]{:S(2)}, u32[]{:S(2)}) collective-permute-start(f32[8,320]{1,0:T(8,128)S(1)} %add.21), channel_id=1, source_target_pairs={{0,8},{1,9},{2,10},{3,11},{4,12},{5,13},{6,14},{7,15},{8,0},{9,1},... | collective-permute-start | bytes 30728 | tf_op jit(solution)/shard_map/ppermute | solution.py:67
  61.6 3.8 %collective-permute-start.12 = (f32[8,320]{1,0:T(8,128)S(1)}, f32[8,320]{1,0:T(8,128)S(1)}, u32[]{:S(2)}, u32[]{:S(2)}) collective-permute-start(f32[8,320]{1,0:T(8,128)S(1)} %add_add_fusion.1), channel_id=1, source_target_pairs={{0,4},{1,5},{2,6},{3,7},{4,0},{5,1},{6,2},{7,3},{8,12},{9,13},{10,... | collective-permute-start | bytes 30728 | tf_op jit(solution)/shard_map/ppermute | solution.py:67
  62.0 3.5 %collective-permute-start.13 = (f32[8,320]{1,0:T(8,128)S(1)}, f32[8,320]{1,0:T(8,128)S(1)}, u32[]{:S(2)}, u32[]{:S(2)}) collective-permute-start(f32[8,320]{1,0:T(8,128)S(1)} %add_add_fusion.1), channel_id=1, source_target_pairs={{0,6},{1,7},{2,4},{3,5},{4,2},{5,3},{6,0},{7,1},{8,14},{9,15},{10,... | collective-permute-start | bytes 30728 | tf_op jit(solution)/shard_map/ppermute | solution.py:67
  62.0 3.5 %collective-permute-start.11 = (f32[8,320]{1,0:T(8,128)S(1)}, f32[8,320]{1,0:T(8,128)S(1)}, u32[]{:S(2)}, u32[]{:S(2)}) collective-permute-start(f32[8,320]{1,0:T(8,128)S(1)} %add_add_fusion.1), channel_id=1, source_target_pairs={{0,2},{1,3},{2,0},{3,1},{4,6},{5,7},{6,4},{7,5},{8,10},{9,11},{10,... | collective-permute-start | bytes 30728 | tf_op jit(solution)/shard_map/ppermute | solution.py:67
where the time goes:
time: 67.5 us; the launch traced here: 67 us
  waiting for transfers between devices  28.2 us (42%)
  starting transfers between devices  26.2 us (39%)
  Pallas kernels  11.3 us (17%)
  between operations  0.74 us (1%)
    ppermute x7, waiting for transfers between devices, shifted(): return lax.ppermute(block, AXES, route)  17.4 us
    ppermute x7, starting transfers between devices, shifted(): return lax.ppermute(block, AXES, route)  15.2 us
    pallas_call x7, Pallas kernels, call(): pl.pallas_call(body, in_specs=[vmem] * len(args) if specs is None else sp...  11.3 us
    ppermute x7, starting transfers between devices, all_sum(): lax.ppermute(part, AXES, [(i, i ^ mask) for i in range(count)])  11 us
    ppermute x7, waiting for transfers between devices, all_sum(): lax.ppermute(part, AXES, [(i, i ^ mask) for i in range(count)])  10.8 us
  transfers between devices with their start and end apart: 14, of which 6 were waited for; matrix products, arithmetic and copies ran while one was open for 1% of the time, Pallas kernels for 12%

commit v1 on v0

--- a/solution.py
+++ b/solution.py
@@ -58,6 +58,7 @@
     count = lax.axis_size(AXES)
     me = lax.axis_index(AXES)
     binary, odd = table_rounds(count)
+    at = 0
     for strides in binary:
         masks = [0]
         for stride in strides:
@@ -65,7 +66,10 @@
         parts = [part]
         for mask in masks[1:]:
             parts.append(lax.ppermute(part, AXES, [(i, i ^ mask) for i in range(count)]))
+        if at == len(binary) - 1 and not odd:
+            return parts
         part = pair_tree(parts)
+        at += 1
     for stride, radix in odd:
         digit = (me // stride) % radix
         parts = [part]
@@ -82,7 +86,8 @@
                 value = jnp.where((digit + step) % radix == d, parts[step], value)
             total = total + value
         part = total
-    return part
+        at += 1
+    return [part]
 
 
 def prep_tiles(head_count, table_ref, chunk_ref, tile_ref):
@@ -357,9 +362,13 @@
         copy.wait()
 
 
-def query_kernel(head_count, dq_ref, one_ref, two_ref, gq_hbm, gq_ref, sems):
+def query_kernel(head_count, dq_ref, one_ref, two_ref, *refs):
+    term_refs = refs[:-5]
+    gq_hbm, table_hbm, gq_ref, table_ref, sems = refs[-5:]
+    table_ref[...] = pair_tree([ref[...] for ref in term_refs])
     head_dim = dq_ref.shape[0] // head_count
-    copies = []
+    copies = [pltpu.make_async_copy(table_ref, table_hbm, sems.at[0])]
+    copies[0].start()
     for head in range(head_count):
         cols = slice(head * head_dim, (head + 1) * head_dim)
         total = dq_ref[cols, :] + one_ref[cols, :].astype(F32) + two_ref[cols, :].astype(F32)
@@ -367,7 +376,7 @@
         if head % 4 == 3:
             part = pl.ds((head - 3) * head_dim, 4 * head_dim)
             copies.append(
-                pltpu.make_async_copy(gq_ref.at[:, part], gq_hbm.at[:, part], sems.at[head // 4])
+                pltpu.make_async_copy(gq_ref.at[:, part], gq_hbm.at[:, part], sems.at[1 + head // 4])
             )
             copies[-1].start()
     for copy in copies:
@@ -462,14 +471,17 @@
         aliases={5: 0, 6: 1, 11: 3},
     )
     back_near = shifted(dq1, 1)
-    grad_table = all_sum(table_part)
+    table_terms = all_sum(table_part)
     grad_key, grad_value = call(
         body(key_value_kernel, head_dim ** (-0.5)), 1, [out_shape] * 2, (dk, dv),
         (rows_b16,) * 2 + (pltpu.SemaphoreType.DMA((2,)),), out_specs=[hbm] * 2,
     )
-    grad_query, = call(
-        body(query_kernel, heads), 1, [out_shape], (dq0, back_near, back_far),
-        (rows_b16, pltpu.SemaphoreType.DMA((heads // 4,))), out_specs=[hbm],
+    table_out = jax.ShapeDtypeStruct((heads, table_len), F32)
+    grad_query, grad_table = call(
+        body(query_kernel, heads), 1, [out_shape, table_out],
+        (dq0, back_near, back_far, *table_terms),
+        (rows_b16, table_shape, pltpu.SemaphoreType.DMA((1 + heads // 4,))),
+        out_specs=[hbm] * 2,
     )
     return grad_query, grad_key, grad_value, grad_table
 

time: 67.5 us -> 67 us (level)
  transfers between devices with their start and end apart: 14 -> 14, of which waited for: 6 -> 6; matrix products, arithmetic and copies ran while one was open for 1% -> 0% of each run, Pallas kernels for 12% -> 12%
where the time goes in v1:
time: 67 us; the launch traced here: 66.5 us
  waiting for transfers between devices  28.5 us (43%)
  starting transfers between devices  25.9 us (39%)
  Pallas kernels  11.3 us (17%)
  between operations  0.76 us (1%)
    ppermute x7, waiting for transfers between devices, shifted(): return lax.ppermute(block, AXES, route)  17.4 us
    ppermute x7, starting transfers between devices, shifted(): return lax.ppermute(block, AXES, route)  15.2 us
    pallas_call x7, Pallas kernels, call(): pl.pallas_call(body, in_specs=[vmem] * len(args) if specs is None else sp...  11.3 us
    ppermute x7, waiting for transfers between devices, all_sum(): lax.ppermute(part, AXES, [(i, i ^ mask) for i in range(count)])  11.1 us
    ppermute x7, starting transfers between devices, all_sum(): lax.ppermute(part, AXES, [(i, i ^ mask) for i in range(count)])  10.7 us
  transfers between devices with their start and end apart: 14, of which 6 were waited for; matrix products, arithmetic and copies ran while one was open for 0% of the time, Pallas kernels for 12%

profile of v1, /device:TPU:0, one launch (start us, length us, event | category | flops | bytes accessed | tf_op | source)
XLA Modules:
  0.0 66.5 jit_solution(8247505712810451730)
XLA Ops:
  0.6 1.3 %shard_map.102 = (bf16[272,1024]{1,0:T(8,128)(2,1)S(1)}, bf16[272,768]{1,0:T(8,128)(2,1)S(1)}, bf16[256,256]{1,0:T(8,128)(2,1)S(1)}, f32[16,256]{1,0:T(8,128)S(1)}) custom-call(bf16[256,1024]{1,0:T(8,128)(2,1)} %g_hbm.1, f32[8,256]{1,0:T(8,128)} %bitcast.2, f32[8,256]{1,0:T(8,128)} %bitcast.3), custom_call_target="tpu_custom_call" | custom-call | flops 16777216 | bytes 2097152 | tf_op jit(solution)/shard_map/pallas_call | solution.py:402
  1.9 1.3 %collective-permute-start.1 = (bf16[272,1024]{1,0:T(8,128)(2,1)S(1)}, bf16[272,1024]{1,0:T(8,128)(2,1)S(1)}, u32[]{:S(2)}, u32[]{:S(2)}) collective-permute-start(bf16[272,1024]{1,0:T(8,128)(2,1)S(1)} %get-tuple-element.34.refs_4_), channel_id=1, source_target_pairs={{2,0},{3,1},{4,2},{5,3},{6,4},{7,5},{8,6},{9,7},{10,8},{11,9},{12,... | collective-permute-start | bytes 1671176 | tf_op jit(solution)/shard_map/ppermute | solution.py:27
  3.2 1.3 %collective-permute-start = (bf16[256,1024]{1,0:T(8,128)(2,1)}, bf16[256,1024]{1,0:T(8,128)(2,1)S(1)}, u32[]{:S(2)}, u32[]{:S(2)}) collective-permute-start(bf16[256,1024]{1,0:T(8,128)(2,1)} %refs_2_.1), channel_id=1, source_target_pairs={{2,0},{3,1},{4,2},{5,3},{6,4},{7,5},{8,6},{9,7},{10,8},{11,9},{12,... | collective-permute-start | bytes 1572872 | tf_op jit(solution)/shard_map/ppermute | solution.py:27
  4.5 1.3 %collective-permute-start.2 = (bf16[256,1024]{1,0:T(8,128)(2,1)}, bf16[256,1024]{1,0:T(8,128)(2,1)S(1)}, u32[]{:S(2)}, u32[]{:S(2)}) collective-permute-start(bf16[256,1024]{1,0:T(8,128)(2,1)} %refs_2_.1), channel_id=1, source_target_pairs={{1,0},{2,1},{3,2},{4,3},{5,4},{6,5},{7,6},{8,7},{9,8},{10,9},{11,1... | collective-permute-start | bytes 1572872 | tf_op jit(solution)/shard_map/ppermute | solution.py:27
  5.8 1.3 %collective-permute-start.3 = (bf16[272,768]{1,0:T(8,128)(2,1)S(1)}, bf16[272,768]{1,0:T(8,128)(2,1)S(1)}, u32[]{:S(2)}, u32[]{:S(2)}) collective-permute-start(bf16[272,768]{1,0:T(8,128)(2,1)S(1)} %get-tuple-element.48), channel_id=1, source_target_pairs={{1,0},{2,1},{3,2},{4,3},{5,4},{6,5},{7,6},{8,7},{9,8},{10,9},{11,1... | collective-permute-start | bytes 1253384 | tf_op jit(solution)/shard_map/ppermute | solution.py:27
  7.1 1.3 %collective-permute-start.4 = (bf16[256,256]{1,0:T(8,128)(2,1)S(1)}, bf16[256,256]{1,0:T(8,128)(2,1)S(1)}, u32[]{:S(2)}, u32[]{:S(2)}) collective-permute-start(bf16[256,256]{1,0:T(8,128)(2,1)S(1)} %get-tuple-element.52), channel_id=1, source_target_pairs={{1,0},{2,1},{3,2},{4,3},{5,4},{6,5},{7,6},{8,7},{9,8},{10,9},{11,1... | collective-permute-start | bytes 393224 | tf_op jit(solution)/shard_map/ppermute | solution.py:27
  8.4 3.6 %shard_map.103 = (f32[1024,256]{1,0:T(8,128)S(1)}, f32[256,1024]{1,0:T(8,128)S(1)}, f32[256,1024]{1,0:T(8,128)S(1)}, f32[8,512]{1,0:T(8,128)S(1)}, bf16[1024,256...) custom-call(bf16[256,1024]{1,0:T(8,128)(2,1)} %refs_0_.1, ...), custom_call_target="tpu_custom_call" | custom-call | flops 671088640 | bytes 2097152 | tf_op jit(solution)/shard_map/pallas_call | solution.py:402
  12.0 0.0 collective-permute-done.refs_8_
  12.0 0.0 collective-permute-done.1.refs_9_
  12.1 2.1 %shard_map.104 = (f32[256,1024]{1,0:T(8,128)S(1)}, f32[256,1024]{1,0:T(8,128)S(1)}, f32[8,512]{1,0:T(8,128)S(1)}, bf16[1024,256]{1,0:T(8,128)(2,1)S(1)}, f32[16,256]{1,0:T(8,128)}) custom-call(bf16[256,1024]{1,0:T(8,128)(2,1)S(1)} %get-tuple-element.37.refs_0_, ...), custom_call_target="tpu_custom_call", output_to_operand_aliasing={{0}: (5, {}), {1}: (6, {}), {2}: (7, {})} | custom-call | flops 671088640 | bytes 2097152 | tf_op jit(solution)/shard_map/pallas_call | solution.py:402
  14.2 16.1 %collective-permute-done.3.refs_9_ = bf16[272,768]{1,0:T(8,128)(2,1)S(1)} collective-permute-done((bf16[272,768]{1,0:T(8,128)(2,1)S(1)}, bf16[272,768]{1,0:T(8,128)(2,1)S(1)}, u32[]{:S(2)}, u32[]{:S(2)}) %collective-permute-start.3) | collective-permute-done | bytes 417824 | tf_op jit(solution)/shard_map/ppermute | solution.py:27
  30.2 1.5 %shard_map.105 = (f32[256,1024]{1,0:T(8,128)S(1)}, f32[256,1024]{1,0:T(8,128)S(1)}, f32[8,512]{1,0:T(8,128)S(1)}, bf16[1024,256]{1,0:T(8,128)(2,1)S(1)}, f32[16,256]{1,0:T(8,128)S(1)}) custom-call(bf16[256,1024]{1,0:T(8,128)(2,1)S(1)} %get-tuple-element.37.refs_0_, ...), custom_call_target="tpu_custom_call", output_to_operand_aliasing={{0}: (5, {}), {1}: (6, {}), {2}: (7, {})} | custom-call | flops 503316480 | bytes 2097152 | tf_op jit(solution)/shard_map/pallas_call | solution.py:402
  31.7 1.3 %collective-permute-done.4.refs_9_ = bf16[256,256]{1,0:T(8,128)(2,1)S(1)} collective-permute-done((bf16[256,256]{1,0:T(8,128)(2,1)S(1)}, bf16[256,256]{1,0:T(8,128)(2,1)S(1)}, u32[]{:S(2)}, u32[]{:S(2)}) %collective-permute-start.4) | collective-permute-done | bytes 131104 | tf_op jit(solution)/shard_map/ppermute | solution.py:27
  33.0 0.8 %shard_map.106 = (f32[256,1024]{1,0:T(8,128)S(1)}, f32[256,1024]{1,0:T(8,128)S(1)}, f32[8,320]{1,0:T(8,128)S(1)}, bf16[1024,256]{1,0:T(8,128)(2,1)S(1)}) custom-call(bf16[256,1024]{1,0:T(8,128)(2,1)S(1)} %get-tuple-element.37.refs_0_, bf16[256,1024]{1,0:T(8,128)(2,1)S(1)} %get-tuple-element.38.refs_1_, ...), custom_call_target="tpu_custom_call", output_to_operand_aliasing={{0}: (5, {}), {1}: (6, {}), {3}: (11, {})} | custom-call | flops 167772160 | bytes 2097152 | tf_op jit(solution)/shard_map/pallas_call | solution.py:402
  33.8 4.6 %collective-permute-start.5 = (bf16[1024,256]{1,0:T(8,128)(2,1)S(1)}, bf16[1024,256]{1,0:T(8,128)(2,1)S(1)}, u32[]{:S(2)}, u32[]{:S(2)}) collective-permute-start(bf16[1024,256]{1,0:T(8,128)(2,1)S(1)} %get-tuple-element.55), channel_id=1, source_target_pairs={{0,1},{1,2},{2,3},{3,4},{4,5},{5,6},{6,7},{7,8},{8,9},{9,10},{10,1... | collective-permute-start | bytes 1572872 | tf_op jit(solution)/shard_map/ppermute | solution.py:27
  38.4 4.2 %collective-permute-start.6 = (bf16[1024,256]{1,0:T(8,128)(2,1)S(1)}, bf16[1024,256]{1,0:T(8,128)(2,1)S(1)}, u32[]{:S(2)}, u32[]{:S(2)}) collective-permute-start(bf16[1024,256]{1,0:T(8,128)(2,1)S(1)} %get-tuple-element.56), channel_id=1, source_target_pairs={{0,2},{1,3},{2,4},{3,5},{4,6},{5,7},{6,8},{7,9},{8,10},{9,11},{10,... | collective-permute-start | bytes 1572872 | tf_op jit(solution)/shard_map/ppermute | solution.py:27
  42.6 0.7 %collective-permute-start.7 = (f32[8,320]{1,0:T(8,128)S(1)}, f32[8,320]{1,0:T(8,128)S(1)}, u32[]{:S(2)}, u32[]{:S(2)}) collective-permute-start(f32[8,320]{1,0:T(8,128)S(1)} %get-tuple-element.57), channel_id=1, source_target_pairs={{0,1},{1,0},{2,3},{3,2},{4,5},{5,4},{6,7},{7,6},{8,9},{9,8},{10,11... | collective-permute-start | bytes 30728 | tf_op jit(solution)/shard_map/ppermute | solution.py:68
  43.2 6.1 %collective-permute-done.7 = f32[8,320]{1,0:T(8,128)S(1)} collective-permute-done((f32[8,320]{1,0:T(8,128)S(1)}, f32[8,320]{1,0:T(8,128)S(1)}, u32[]{:S(2)}, u32[]{:S(2)}) %collective-permute-start.7) | collective-permute-done | bytes 10272 | tf_op jit(solution)/shard_map/ppermute | solution.py:68
  49.4 6.8 %collective-permute-start.9 = (f32[8,320]{1,0:T(8,128)S(1)}, f32[8,320]{1,0:T(8,128)S(1)}, u32[]{:S(2)}, u32[]{:S(2)}) collective-permute-start(f32[8,320]{1,0:T(8,128)S(1)} %add.12), channel_id=1, source_target_pairs={{0,16},{1,17},{2,18},{3,19},{4,20},{5,21},{6,22},{7,23},{8,24},{9,... | collective-permute-start | bytes 30728 | tf_op jit(solution)/shard_map/ppermute | solution.py:68
  56.1 1.3 %collective-permute-start.10 = (f32[8,320]{1,0:T(8,128)S(1)}, f32[8,320]{1,0:T(8,128)S(1)}, u32[]{:S(2)}, u32[]{:S(2)}) collective-permute-start(f32[8,320]{1,0:T(8,128)S(1)} %add.12), channel_id=1, source_target_pairs={{0,24},{1,25},{2,26},{3,27},{4,28},{5,29},{6,30},{7,31},{8,16},{9,... | collective-permute-start | bytes 30728 | tf_op jit(solution)/shard_map/ppermute | solution.py:68
  57.5 0.3 collective-permute-done.9
  57.8 3.8 %collective-permute-done.10 = f32[8,320]{1,0:T(8,128)S(1)} collective-permute-done((f32[8,320]{1,0:T(8,128)S(1)}, f32[8,320]{1,0:T(8,128)S(1)}, u32[]{:S(2)}, u32[]{:S(2)}) %collective-permute-start.10) | collective-permute-done | bytes 10272 | tf_op jit(solution)/shard_map/ppermute | solution.py:68
  61.6 0.0 collective-permute-done.8
  61.6 0.1 collective-permute-start.11
  61.7 0.3 collective-permute-start.12
  62.0 1.5 %collective-permute-start.13 = (f32[8,320]{1,0:T(8,128)S(1)}, f32[8,320]{1,0:T(8,128)S(1)}, u32[]{:S(2)}, u32[]{:S(2)}) collective-permute-start(f32[8,320]{1,0:T(8,128)S(1)} %add_add_fusion.refs_0_), channel_id=1, source_target_pairs={{0,6},{1,7},{2,4},{3,5},{4,2},{5,3},{6,0},{7,1},{8,14},{9,15},{10,... | collective-permute-start | bytes 30728 | tf_op jit(solution)/shard_map/ppermute | solution.py:68
  63.6 1.1 %shard_map.108 = (bf16[256,1024]{1,0:T(8,128)(2,1)}, bf16[256,1024]{1,0:T(8,128)(2,1)}) custom-call(f32[256,1024]{1,0:T(8,128)S(1)} %get-tuple-element.59.dk_ref, f32[256,1024]{1,0:T(8,128)S(1)} %get-tuple-element.60.dv_ref), custom_call_target="tpu_custom_call" | custom-call | flops 16777216 | bytes 2097152 | tf_op jit(solution)/shard_map/pallas_call | solution.py:402
  64.6 0.0 collective-permute-done.11.refs_1_
  64.7 0.8 %collective-permute-done.12.refs_2_ = f32[8,320]{1,0:T(8,128)S(1)} collective-permute-done((f32[8,320]{1,0:T(8,128)S(1)}, f32[8,320]{1,0:T(8,128)S(1)}, u32[]{:S(2)}, u32[]{:S(2)}) %collective-permute-start.12) | collective-permute-done | bytes 10272 | tf_op jit(solution)/shard_map/ppermute | solution.py:68
  65.5 0.0 collective-permute-done.13.refs_3_
  65.5 0.0 collective-permute-done.5.one_ref
  65.5 1.0 %shard_map.107 = (bf16[256,1024]{1,0:T(8,128)(2,1)}, f32[8,320]{1,0:T(8,128)}) custom-call(f32[1024,256]{1,0:T(8,128)S(1)} %get-tuple-element.36.dq_ref, bf16[1024,256]{1,0:T(8,128)(2,1)S(1)} %collective-permute-done.5.one_ref, bf16[1024,256]{1,0:T(8,128)(2,1)S(1)} %collective-permute-done.6.two_ref, f32[8,320]{1,0:T(8,128)S(1)} %add_add_fusion.refs_0_, ...), custom_call_target="tpu_custom_call" | custom-call | flops 16777216 | bytes 2097152 | tf_op jit(solution)/shard_map/pallas_call | solution.py:402
  (5 shorter events, 0.0 us)
Async XLA Ops:
  1.9 10.2 %collective-permute-start.1 = (bf16[272,1024]{1,0:T(8,128)(2,1)S(1)}, bf16[272,1024]{1,0:T(8,128)(2,1)S(1)}, u32[]{:S(2)}, u32[]{:S(2)}) collective-permute-start(bf16[272,1024]{1,0:T(8,128)(2,1)S(1)} %get-tuple-element.34.refs_4_), channel_id=1, source_target_pairs={{2,0},{3,1},{4,2},{5,3},{6,4},{7,5},{8,6},{9,7},{10,8},{11,9},{12,... | collective-permute-start | bytes 1671176 | tf_op jit(solution)/shard_map/ppermute | solution.py:27
  3.2 8.8 %collective-permute-start = (bf16[256,1024]{1,0:T(8,128)(2,1)}, bf16[256,1024]{1,0:T(8,128)(2,1)S(1)}, u32[]{:S(2)}, u32[]{:S(2)}) collective-permute-start(bf16[256,1024]{1,0:T(8,128)(2,1)} %refs_2_.1), channel_id=1, source_target_pairs={{2,0},{3,1},{4,2},{5,3},{6,4},{7,5},{8,6},{9,7},{10,8},{11,9},{12,... | collective-permute-start | bytes 1572872 | tf_op jit(solution)/shard_map/ppermute | solution.py:27
  4.5 25.7 %collective-permute-start.2 = (bf16[256,1024]{1,0:T(8,128)(2,1)}, bf16[256,1024]{1,0:T(8,128)(2,1)S(1)}, u32[]{:S(2)}, u32[]{:S(2)}) collective-permute-start(bf16[256,1024]{1,0:T(8,128)(2,1)} %refs_2_.1), channel_id=1, source_target_pairs={{1,0},{2,1},{3,2},{4,3},{5,4},{6,5},{7,6},{8,7},{9,8},{10,9},{11,1... | collective-permute-start | bytes 1572872 | tf_op jit(solution)/shard_map/ppermute | solution.py:27
  5.8 24.4 %collective-permute-start.3 = (bf16[272,768]{1,0:T(8,128)(2,1)S(1)}, bf16[272,768]{1,0:T(8,128)(2,1)S(1)}, u32[]{:S(2)}, u32[]{:S(2)}) collective-permute-start(bf16[272,768]{1,0:T(8,128)(2,1)S(1)} %get-tuple-element.48), channel_id=1, source_target_pairs={{1,0},{2,1},{3,2},{4,3},{5,4},{6,5},{7,6},{8,7},{9,8},{10,9},{11,1... | collective-permute-start | bytes 1253384 | tf_op jit(solution)/shard_map/ppermute | solution.py:27
  7.1 26.0 %collective-permute-start.4 = (bf16[256,256]{1,0:T(8,128)(2,1)S(1)}, bf16[256,256]{1,0:T(8,128)(2,1)S(1)}, u32[]{:S(2)}, u32[]{:S(2)}) collective-permute-start(bf16[256,256]{1,0:T(8,128)(2,1)S(1)} %get-tuple-element.52), channel_id=1, source_target_pairs={{1,0},{2,1},{3,2},{4,3},{5,4},{6,5},{7,6},{8,7},{9,8},{10,9},{11,1... | collective-permute-start | bytes 393224 | tf_op jit(solution)/shard_map/ppermute | solution.py:27
  33.8 31.7 %collective-permute-start.5 = (bf16[1024,256]{1,0:T(8,128)(2,1)S(1)}, bf16[1024,256]{1,0:T(8,128)(2,1)S(1)}, u32[]{:S(2)}, u32[]{:S(2)}) collective-permute-start(bf16[1024,256]{1,0:T(8,128)(2,1)S(1)} %get-tuple-element.55), channel_id=1, source_target_pairs={{0,1},{1,2},{2,3},{3,4},{4,5},{5,6},{6,7},{7,8},{8,9},{9,10},{10,1... | collective-permute-start | bytes 1572872 | tf_op jit(solution)/shard_map/ppermute | solution.py:27
  38.4 27.1 %collective-permute-start.6 = (bf16[1024,256]{1,0:T(8,128)(2,1)S(1)}, bf16[1024,256]{1,0:T(8,128)(2,1)S(1)}, u32[]{:S(2)}, u32[]{:S(2)}) collective-permute-start(bf16[1024,256]{1,0:T(8,128)(2,1)S(1)} %get-tuple-element.56), channel_id=1, source_target_pairs={{0,2},{1,3},{2,4},{3,5},{4,6},{5,7},{6,8},{7,9},{8,10},{9,11},{10,... | collective-permute-start | bytes 1572872 | tf_op jit(solution)/shard_map/ppermute | solution.py:27
  42.6 6.8 %collective-permute-start.7 = (f32[8,320]{1,0:T(8,128)S(1)}, f32[8,320]{1,0:T(8,128)S(1)}, u32[]{:S(2)}, u32[]{:S(2)}) collective-permute-start(f32[8,320]{1,0:T(8,128)S(1)} %get-tuple-element.57), channel_id=1, source_target_pairs={{0,1},{1,0},{2,3},{3,2},{4,5},{5,4},{6,7},{7,6},{8,9},{9,8},{10,11... | collective-permute-start | bytes 30728 | tf_op jit(solution)/shard_map/ppermute | solution.py:68
  49.4 8.5 %collective-permute-start.9 = (f32[8,320]{1,0:T(8,128)S(1)}, f32[8,320]{1,0:T(8,128)S(1)}, u32[]{:S(2)}, u32[]{:S(2)}) collective-permute-start(f32[8,320]{1,0:T(8,128)S(1)} %add.12), channel_id=1, source_target_pairs={{0,16},{1,17},{2,18},{3,19},{4,20},{5,21},{6,22},{7,23},{8,24},{9,... | collective-permute-start | bytes 30728 | tf_op jit(solution)/shard_map/ppermute | solution.py:68
  56.1 5.5 %collective-permute-start.10 = (f32[8,320]{1,0:T(8,128)S(1)}, f32[8,320]{1,0:T(8,128)S(1)}, u32[]{:S(2)}, u32[]{:S(2)}) collective-permute-start(f32[8,320]{1,0:T(8,128)S(1)} %add.12), channel_id=1, source_target_pairs={{0,24},{1,25},{2,26},{3,27},{4,28},{5,29},{6,30},{7,31},{8,16},{9,... | collective-permute-start | bytes 30728 | tf_op jit(solution)/shard_map/ppermute | solution.py:68
  57.5 4.1 %collective-permute-start.8 = (f32[8,320]{1,0:T(8,128)S(1)}, f32[8,320]{1,0:T(8,128)S(1)}, u32[]{:S(2)}, u32[]{:S(2)}) collective-permute-start(f32[8,320]{1,0:T(8,128)S(1)} %add.12), channel_id=1, source_target_pairs={{0,8},{1,9},{2,10},{3,11},{4,12},{5,13},{6,14},{7,15},{8,0},{9,1},... | collective-permute-start | bytes 30728 | tf_op jit(solution)/shard_map/ppermute | solution.py:68
  61.6 3.0 %collective-permute-start.11 = (f32[8,320]{1,0:T(8,128)S(1)}, f32[8,320]{1,0:T(8,128)S(1)}, u32[]{:S(2)}, u32[]{:S(2)}) collective-permute-start(f32[8,320]{1,0:T(8,128)S(1)} %add_add_fusion.refs_0_), channel_id=1, source_target_pairs={{0,2},{1,3},{2,0},{3,1},{4,6},{5,7},{6,4},{7,5},{8,10},{9,11},{10,... | collective-permute-start | bytes 30728 | tf_op jit(solution)/shard_map/ppermute | solution.py:68
  61.7 3.8 %collective-permute-start.12 = (f32[8,320]{1,0:T(8,128)S(1)}, f32[8,320]{1,0:T(8,128)S(1)}, u32[]{:S(2)}, u32[]{:S(2)}) collective-permute-start(f32[8,320]{1,0:T(8,128)S(1)} %add_add_fusion.refs_0_), channel_id=1, source_target_pairs={{0,4},{1,5},{2,6},{3,7},{4,0},{5,1},{6,2},{7,3},{8,12},{9,13},{10,... | collective-permute-start | bytes 30728 | tf_op jit(solution)/shard_map/ppermute | solution.py:68
  62.0 3.5 %collective-permute-start.13 = (f32[8,320]{1,0:T(8,128)S(1)}, f32[8,320]{1,0:T(8,128)S(1)}, u32[]{:S(2)}, u32[]{:S(2)}) collective-permute-start(f32[8,320]{1,0:T(8,128)S(1)} %add_add_fusion.refs_0_), channel_id=1, source_target_pairs={{0,6},{1,7},{2,4},{3,5},{4,2},{5,3},{6,0},{7,1},{8,14},{9,15},{10,... | collective-permute-start | bytes 30728 | tf_op jit(solution)/shard_map/ppermute | solution.py:68

commit v2 on v1

--- a/solution.py
+++ b/solution.py
@@ -372,11 +372,11 @@
     for head in range(head_count):
         cols = slice(head * head_dim, (head + 1) * head_dim)
         total = dq_ref[cols, :] + one_ref[cols, :].astype(F32) + two_ref[cols, :].astype(F32)
-        gq_ref[:, cols] = total.T.astype(BF16)
-        if head % 4 == 3:
-            part = pl.ds((head - 3) * head_dim, 4 * head_dim)
+        gq_ref[:, cols] = total.astype(BF16).T
+        if head % 2 == 1:
+            part = pl.ds((head - 1) * head_dim, 2 * head_dim)
             copies.append(
-                pltpu.make_async_copy(gq_ref.at[:, part], gq_hbm.at[:, part], sems.at[1 + head // 4])
+                pltpu.make_async_copy(gq_ref.at[:, part], gq_hbm.at[:, part], sems.at[1 + head // 2])
             )
             copies[-1].start()
     for copy in copies:
@@ -480,7 +480,7 @@
     grad_query, grad_table = call(
         body(query_kernel, heads), 1, [out_shape, table_out],
         (dq0, back_near, back_far, *table_terms),
-        (rows_b16, table_shape, pltpu.SemaphoreType.DMA((1 + heads // 4,))),
+        (rows_b16, table_shape, pltpu.SemaphoreType.DMA((1 + heads // 2,))),
         out_specs=[hbm] * 2,
     )
     return grad_query, grad_key, grad_value, grad_table

time: 67 us -> 66.9 us (level)
  no operation moved by 1% of the time
where the time goes in v2:
time: 66.9 us; the launch traced here: 66.4 us
  waiting for transfers between devices  28.5 us (43%)
  starting transfers between devices  25.9 us (39%)
  Pallas kernels  11.3 us (17%)
  between operations  0.76 us (1%)
    ppermute x7, waiting for transfers between devices, shifted(): return lax.ppermute(block, AXES, route)  17.4 us
    ppermute x7, starting transfers between devices, shifted(): return lax.ppermute(block, AXES, route)  15.2 us
    pallas_call x7, Pallas kernels, call(): pl.pallas_call(body, in_specs=[vmem] * len(args) if specs is None else sp...  11.3 us
    ppermute x7, waiting for transfers between devices, all_sum(): lax.ppermute(part, AXES, [(i, i ^ mask) for i in range(count)])  11.1 us
    ppermute x7, starting transfers between devices, all_sum(): lax.ppermute(part, AXES, [(i, i ^ mask) for i in range(count)])  10.7 us
  transfers between devices with their start and end apart: 14, of which 6 were waited for; matrix products, arithmetic and copies ran while one was open for 0% of the time, Pallas kernels for 12%

profile of v2, /device:TPU:0, one launch (start us, length us, event | category | flops | bytes accessed | tf_op | source)
XLA Modules:
  0.0 66.4 jit_solution(2092770669158540445)
XLA Ops:
  0.6 1.3 %shard_map.102 = (bf16[272,1024]{1,0:T(8,128)(2,1)S(1)}, bf16[272,768]{1,0:T(8,128)(2,1)S(1)}, bf16[256,256]{1,0:T(8,128)(2,1)S(1)}, f32[16,256]{1,0:T(8,128)S(1)}) custom-call(bf16[256,1024]{1,0:T(8,128)(2,1)} %g_hbm.1, f32[8,256]{1,0:T(8,128)} %bitcast.2, f32[8,256]{1,0:T(8,128)} %bitcast.3), custom_call_target="tpu_custom_call" | custom-call | flops 16777216 | bytes 2097152 | tf_op jit(solution)/shard_map/pallas_call | solution.py:402
  1.9 1.3 %collective-permute-start.1 = (bf16[272,1024]{1,0:T(8,128)(2,1)S(1)}, bf16[272,1024]{1,0:T(8,128)(2,1)S(1)}, u32[]{:S(2)}, u32[]{:S(2)}) collective-permute-start(bf16[272,1024]{1,0:T(8,128)(2,1)S(1)} %get-tuple-element.34.refs_4_), channel_id=1, source_target_pairs={{2,0},{3,1},{4,2},{5,3},{6,4},{7,5},{8,6},{9,7},{10,8},{11,9},{12,... | collective-permute-start | bytes 1671176 | tf_op jit(solution)/shard_map/ppermute | solution.py:27
  3.2 1.3 %collective-permute-start = (bf16[256,1024]{1,0:T(8,128)(2,1)}, bf16[256,1024]{1,0:T(8,128)(2,1)S(1)}, u32[]{:S(2)}, u32[]{:S(2)}) collective-permute-start(bf16[256,1024]{1,0:T(8,128)(2,1)} %refs_2_.1), channel_id=1, source_target_pairs={{2,0},{3,1},{4,2},{5,3},{6,4},{7,5},{8,6},{9,7},{10,8},{11,9},{12,... | collective-permute-start | bytes 1572872 | tf_op jit(solution)/shard_map/ppermute | solution.py:27
  4.5 1.3 %collective-permute-start.2 = (bf16[256,1024]{1,0:T(8,128)(2,1)}, bf16[256,1024]{1,0:T(8,128)(2,1)S(1)}, u32[]{:S(2)}, u32[]{:S(2)}) collective-permute-start(bf16[256,1024]{1,0:T(8,128)(2,1)} %refs_2_.1), channel_id=1, source_target_pairs={{1,0},{2,1},{3,2},{4,3},{5,4},{6,5},{7,6},{8,7},{9,8},{10,9},{11,1... | collective-permute-start | bytes 1572872 | tf_op jit(solution)/shard_map/ppermute | solution.py:27
  5.8 1.3 %collective-permute-start.3 = (bf16[272,768]{1,0:T(8,128)(2,1)S(1)}, bf16[272,768]{1,0:T(8,128)(2,1)S(1)}, u32[]{:S(2)}, u32[]{:S(2)}) collective-permute-start(bf16[272,768]{1,0:T(8,128)(2,1)S(1)} %get-tuple-element.48), channel_id=1, source_target_pairs={{1,0},{2,1},{3,2},{4,3},{5,4},{6,5},{7,6},{8,7},{9,8},{10,9},{11,1... | collective-permute-start | bytes 1253384 | tf_op jit(solution)/shard_map/ppermute | solution.py:27
  7.1 1.3 %collective-permute-start.4 = (bf16[256,256]{1,0:T(8,128)(2,1)S(1)}, bf16[256,256]{1,0:T(8,128)(2,1)S(1)}, u32[]{:S(2)}, u32[]{:S(2)}) collective-permute-start(bf16[256,256]{1,0:T(8,128)(2,1)S(1)} %get-tuple-element.52), channel_id=1, source_target_pairs={{1,0},{2,1},{3,2},{4,3},{5,4},{6,5},{7,6},{8,7},{9,8},{10,9},{11,1... | collective-permute-start | bytes 393224 | tf_op jit(solution)/shard_map/ppermute | solution.py:27
  8.4 3.6 %shard_map.103 = (f32[1024,256]{1,0:T(8,128)S(1)}, f32[256,1024]{1,0:T(8,128)S(1)}, f32[256,1024]{1,0:T(8,128)S(1)}, f32[8,512]{1,0:T(8,128)S(1)}, bf16[1024,256...) custom-call(bf16[256,1024]{1,0:T(8,128)(2,1)} %refs_0_.1, ...), custom_call_target="tpu_custom_call" | custom-call | flops 671088640 | bytes 2097152 | tf_op jit(solution)/shard_map/pallas_call | solution.py:402
  12.0 0.0 collective-permute-done.refs_8_
  12.0 0.0 collective-permute-done.1.refs_9_
  12.1 2.1 %shard_map.104 = (f32[256,1024]{1,0:T(8,128)S(1)}, f32[256,1024]{1,0:T(8,128)S(1)}, f32[8,512]{1,0:T(8,128)S(1)}, bf16[1024,256]{1,0:T(8,128)(2,1)S(1)}, f32[16,256]{1,0:T(8,128)}) custom-call(bf16[256,1024]{1,0:T(8,128)(2,1)S(1)} %get-tuple-element.37.refs_0_, ...), custom_call_target="tpu_custom_call", output_to_operand_aliasing={{0}: (5, {}), {1}: (6, {}), {2}: (7, {})} | custom-call | flops 671088640 | bytes 2097152 | tf_op jit(solution)/shard_map/pallas_call | solution.py:402
  14.2 16.1 %collective-permute-done.3.refs_9_ = bf16[272,768]{1,0:T(8,128)(2,1)S(1)} collective-permute-done((bf16[272,768]{1,0:T(8,128)(2,1)S(1)}, bf16[272,768]{1,0:T(8,128)(2,1)S(1)}, u32[]{:S(2)}, u32[]{:S(2)}) %collective-permute-start.3) | collective-permute-done | bytes 417824 | tf_op jit(solution)/shard_map/ppermute | solution.py:27
  30.2 1.5 %shard_map.105 = (f32[256,1024]{1,0:T(8,128)S(1)}, f32[256,1024]{1,0:T(8,128)S(1)}, f32[8,512]{1,0:T(8,128)S(1)}, bf16[1024,256]{1,0:T(8,128)(2,1)S(1)}, f32[16,256]{1,0:T(8,128)S(1)}) custom-call(bf16[256,1024]{1,0:T(8,128)(2,1)S(1)} %get-tuple-element.37.refs_0_, ...), custom_call_target="tpu_custom_call", output_to_operand_aliasing={{0}: (5, {}), {1}: (6, {}), {2}: (7, {})} | custom-call | flops 503316480 | bytes 2097152 | tf_op jit(solution)/shard_map/pallas_call | solution.py:402
  31.7 1.3 %collective-permute-done.4.refs_9_ = bf16[256,256]{1,0:T(8,128)(2,1)S(1)} collective-permute-done((bf16[256,256]{1,0:T(8,128)(2,1)S(1)}, bf16[256,256]{1,0:T(8,128)(2,1)S(1)}, u32[]{:S(2)}, u32[]{:S(2)}) %collective-permute-start.4) | collective-permute-done | bytes 131104 | tf_op jit(solution)/shard_map/ppermute | solution.py:27
  33.0 0.8 %shard_map.106 = (f32[256,1024]{1,0:T(8,128)S(1)}, f32[256,1024]{1,0:T(8,128)S(1)}, f32[8,320]{1,0:T(8,128)S(1)}, bf16[1024,256]{1,0:T(8,128)(2,1)S(1)}) custom-call(bf16[256,1024]{1,0:T(8,128)(2,1)S(1)} %get-tuple-element.37.refs_0_, bf16[256,1024]{1,0:T(8,128)(2,1)S(1)} %get-tuple-element.38.refs_1_, ...), custom_call_target="tpu_custom_call", output_to_operand_aliasing={{0}: (5, {}), {1}: (6, {}), {3}: (11, {})} | custom-call | flops 167772160 | bytes 2097152 | tf_op jit(solution)/shard_map/pallas_call | solution.py:402
  33.8 4.6 %collective-permute-start.5 = (bf16[1024,256]{1,0:T(8,128)(2,1)S(1)}, bf16[1024,256]{1,0:T(8,128)(2,1)S(1)}, u32[]{:S(2)}, u32[]{:S(2)}) collective-permute-start(bf16[1024,256]{1,0:T(8,128)(2,1)S(1)} %get-tuple-element.55), channel_id=1, source_target_pairs={{0,1},{1,2},{2,3},{3,4},{4,5},{5,6},{6,7},{7,8},{8,9},{9,10},{10,1... | collective-permute-start | bytes 1572872 | tf_op jit(solution)/shard_map/ppermute | solution.py:27
  38.4 4.2 %collective-permute-start.6 = (bf16[1024,256]{1,0:T(8,128)(2,1)S(1)}, bf16[1024,256]{1,0:T(8,128)(2,1)S(1)}, u32[]{:S(2)}, u32[]{:S(2)}) collective-permute-start(bf16[1024,256]{1,0:T(8,128)(2,1)S(1)} %get-tuple-element.56), channel_id=1, source_target_pairs={{0,2},{1,3},{2,4},{3,5},{4,6},{5,7},{6,8},{7,9},{8,10},{9,11},{10,... | collective-permute-start | bytes 1572872 | tf_op jit(solution)/shard_map/ppermute | solution.py:27
  42.6 0.7 %collective-permute-start.7 = (f32[8,320]{1,0:T(8,128)S(1)}, f32[8,320]{1,0:T(8,128)S(1)}, u32[]{:S(2)}, u32[]{:S(2)}) collective-permute-start(f32[8,320]{1,0:T(8,128)S(1)} %get-tuple-element.57), channel_id=1, source_target_pairs={{0,1},{1,0},{2,3},{3,2},{4,5},{5,4},{6,7},{7,6},{8,9},{9,8},{10,11... | collective-permute-start | bytes 30728 | tf_op jit(solution)/shard_map/ppermute | solution.py:68
  43.2 6.1 %collective-permute-done.7 = f32[8,320]{1,0:T(8,128)S(1)} collective-permute-done((f32[8,320]{1,0:T(8,128)S(1)}, f32[8,320]{1,0:T(8,128)S(1)}, u32[]{:S(2)}, u32[]{:S(2)}) %collective-permute-start.7) | collective-permute-done | bytes 10272 | tf_op jit(solution)/shard_map/ppermute | solution.py:68
  49.4 6.8 %collective-permute-start.9 = (f32[8,320]{1,0:T(8,128)S(1)}, f32[8,320]{1,0:T(8,128)S(1)}, u32[]{:S(2)}, u32[]{:S(2)}) collective-permute-start(f32[8,320]{1,0:T(8,128)S(1)} %add.12), channel_id=1, source_target_pairs={{0,16},{1,17},{2,18},{3,19},{4,20},{5,21},{6,22},{7,23},{8,24},{9,... | collective-permute-start | bytes 30728 | tf_op jit(solution)/shard_map/ppermute | solution.py:68
  56.1 1.3 %collective-permute-start.10 = (f32[8,320]{1,0:T(8,128)S(1)}, f32[8,320]{1,0:T(8,128)S(1)}, u32[]{:S(2)}, u32[]{:S(2)}) collective-permute-start(f32[8,320]{1,0:T(8,128)S(1)} %add.12), channel_id=1, source_target_pairs={{0,24},{1,25},{2,26},{3,27},{4,28},{5,29},{6,30},{7,31},{8,16},{9,... | collective-permute-start | bytes 30728 | tf_op jit(solution)/shard_map/ppermute | solution.py:68
  57.5 0.3 collective-permute-done.9
  57.8 3.8 %collective-permute-done.10 = f32[8,320]{1,0:T(8,128)S(1)} collective-permute-done((f32[8,320]{1,0:T(8,128)S(1)}, f32[8,320]{1,0:T(8,128)S(1)}, u32[]{:S(2)}, u32[]{:S(2)}) %collective-permute-start.10) | collective-permute-done | bytes 10272 | tf_op jit(solution)/shard_map/ppermute | solution.py:68
  61.6 0.0 collective-permute-done.8
  61.6 0.1 collective-permute-start.11
  61.7 0.3 collective-permute-start.12
  62.0 1.5 %collective-permute-start.13 = (f32[8,320]{1,0:T(8,128)S(1)}, f32[8,320]{1,0:T(8,128)S(1)}, u32[]{:S(2)}, u32[]{:S(2)}) collective-permute-start(f32[8,320]{1,0:T(8,128)S(1)} %add_add_fusion.refs_0_), channel_id=1, source_target_pairs={{0,6},{1,7},{2,4},{3,5},{4,2},{5,3},{6,0},{7,1},{8,14},{9,15},{10,... | collective-permute-start | bytes 30728 | tf_op jit(solution)/shard_map/ppermute | solution.py:68
  63.6 1.1 %shard_map.108 = (bf16[256,1024]{1,0:T(8,128)(2,1)}, bf16[256,1024]{1,0:T(8,128)(2,1)}) custom-call(f32[256,1024]{1,0:T(8,128)S(1)} %get-tuple-element.59.dk_ref, f32[256,1024]{1,0:T(8,128)S(1)} %get-tuple-element.60.dv_ref), custom_call_target="tpu_custom_call" | custom-call | flops 16777216 | bytes 2097152 | tf_op jit(solution)/shard_map/pallas_call | solution.py:402
  64.6 0.0 collective-permute-done.11.refs_1_
  64.7 0.8 %collective-permute-done.12.refs_2_ = f32[8,320]{1,0:T(8,128)S(1)} collective-permute-done((f32[8,320]{1,0:T(8,128)S(1)}, f32[8,320]{1,0:T(8,128)S(1)}, u32[]{:S(2)}, u32[]{:S(2)}) %collective-permute-start.12) | collective-permute-done | bytes 10272 | tf_op jit(solution)/shard_map/ppermute | solution.py:68
  65.5 0.0 collective-permute-done.13.refs_3_
  65.5 0.0 collective-permute-done.5.one_ref
  65.5 0.9 %shard_map.107 = (bf16[256,1024]{1,0:T(8,128)(2,1)}, f32[8,320]{1,0:T(8,128)}) custom-call(f32[1024,256]{1,0:T(8,128)S(1)} %get-tuple-element.36.dq_ref, bf16[1024,256]{1,0:T(8,128)(2,1)S(1)} %collective-permute-done.5.one_ref, bf16[1024,256]{1,0:T(8,128)(2,1)S(1)} %collective-permute-done.6.two_ref, f32[8,320]{1,0:T(8,128)S(1)} %add_add_fusion.refs_0_, ...), custom_call_target="tpu_custom_call" | custom-call | flops 16777216 | bytes 2097152 | tf_op jit(solution)/shard_map/pallas_call | solution.py:402
  (5 shorter events, 0.0 us)
Async XLA Ops:
  1.9 10.2 %collective-permute-start.1 = (bf16[272,1024]{1,0:T(8,128)(2,1)S(1)}, bf16[272,1024]{1,0:T(8,128)(2,1)S(1)}, u32[]{:S(2)}, u32[]{:S(2)}) collective-permute-start(bf16[272,1024]{1,0:T(8,128)(2,1)S(1)} %get-tuple-element.34.refs_4_), channel_id=1, source_target_pairs={{2,0},{3,1},{4,2},{5,3},{6,4},{7,5},{8,6},{9,7},{10,8},{11,9},{12,... | collective-permute-start | bytes 1671176 | tf_op jit(solution)/shard_map/ppermute | solution.py:27
  3.2 8.8 %collective-permute-start = (bf16[256,1024]{1,0:T(8,128)(2,1)}, bf16[256,1024]{1,0:T(8,128)(2,1)S(1)}, u32[]{:S(2)}, u32[]{:S(2)}) collective-permute-start(bf16[256,1024]{1,0:T(8,128)(2,1)} %refs_2_.1), channel_id=1, source_target_pairs={{2,0},{3,1},{4,2},{5,3},{6,4},{7,5},{8,6},{9,7},{10,8},{11,9},{12,... | collective-permute-start | bytes 1572872 | tf_op jit(solution)/shard_map/ppermute | solution.py:27
  4.5 25.7 %collective-permute-start.2 = (bf16[256,1024]{1,0:T(8,128)(2,1)}, bf16[256,1024]{1,0:T(8,128)(2,1)S(1)}, u32[]{:S(2)}, u32[]{:S(2)}) collective-permute-start(bf16[256,1024]{1,0:T(8,128)(2,1)} %refs_2_.1), channel_id=1, source_target_pairs={{1,0},{2,1},{3,2},{4,3},{5,4},{6,5},{7,6},{8,7},{9,8},{10,9},{11,1... | collective-permute-start | bytes 1572872 | tf_op jit(solution)/shard_map/ppermute | solution.py:27
  5.8 24.4 %collective-permute-start.3 = (bf16[272,768]{1,0:T(8,128)(2,1)S(1)}, bf16[272,768]{1,0:T(8,128)(2,1)S(1)}, u32[]{:S(2)}, u32[]{:S(2)}) collective-permute-start(bf16[272,768]{1,0:T(8,128)(2,1)S(1)} %get-tuple-element.48), channel_id=1, source_target_pairs={{1,0},{2,1},{3,2},{4,3},{5,4},{6,5},{7,6},{8,7},{9,8},{10,9},{11,1... | collective-permute-start | bytes 1253384 | tf_op jit(solution)/shard_map/ppermute | solution.py:27
  7.1 26.0 %collective-permute-start.4 = (bf16[256,256]{1,0:T(8,128)(2,1)S(1)}, bf16[256,256]{1,0:T(8,128)(2,1)S(1)}, u32[]{:S(2)}, u32[]{:S(2)}) collective-permute-start(bf16[256,256]{1,0:T(8,128)(2,1)S(1)} %get-tuple-element.52), channel_id=1, source_target_pairs={{1,0},{2,1},{3,2},{4,3},{5,4},{6,5},{7,6},{8,7},{9,8},{10,9},{11,1... | collective-permute-start | bytes 393224 | tf_op jit(solution)/shard_map/ppermute | solution.py:27
  33.8 31.7 %collective-permute-start.5 = (bf16[1024,256]{1,0:T(8,128)(2,1)S(1)}, bf16[1024,256]{1,0:T(8,128)(2,1)S(1)}, u32[]{:S(2)}, u32[]{:S(2)}) collective-permute-start(bf16[1024,256]{1,0:T(8,128)(2,1)S(1)} %get-tuple-element.55), channel_id=1, source_target_pairs={{0,1},{1,2},{2,3},{3,4},{4,5},{5,6},{6,7},{7,8},{8,9},{9,10},{10,1... | collective-permute-start | bytes 1572872 | tf_op jit(solution)/shard_map/ppermute | solution.py:27
  38.4 27.1 %collective-permute-start.6 = (bf16[1024,256]{1,0:T(8,128)(2,1)S(1)}, bf16[1024,256]{1,0:T(8,128)(2,1)S(1)}, u32[]{:S(2)}, u32[]{:S(2)}) collective-permute-start(bf16[1024,256]{1,0:T(8,128)(2,1)S(1)} %get-tuple-element.56), channel_id=1, source_target_pairs={{0,2},{1,3},{2,4},{3,5},{4,6},{5,7},{6,8},{7,9},{8,10},{9,11},{10,... | collective-permute-start | bytes 1572872 | tf_op jit(solution)/shard_map/ppermute | solution.py:27
  42.6 6.8 %collective-permute-start.7 = (f32[8,320]{1,0:T(8,128)S(1)}, f32[8,320]{1,0:T(8,128)S(1)}, u32[]{:S(2)}, u32[]{:S(2)}) collective-permute-start(f32[8,320]{1,0:T(8,128)S(1)} %get-tuple-element.57), channel_id=1, source_target_pairs={{0,1},{1,0},{2,3},{3,2},{4,5},{5,4},{6,7},{7,6},{8,9},{9,8},{10,11... | collective-permute-start | bytes 30728 | tf_op jit(solution)/shard_map/ppermute | solution.py:68
  49.4 8.5 %collective-permute-start.9 = (f32[8,320]{1,0:T(8,128)S(1)}, f32[8,320]{1,0:T(8,128)S(1)}, u32[]{:S(2)}, u32[]{:S(2)}) collective-permute-start(f32[8,320]{1,0:T(8,128)S(1)} %add.12), channel_id=1, source_target_pairs={{0,16},{1,17},{2,18},{3,19},{4,20},{5,21},{6,22},{7,23},{8,24},{9,... | collective-permute-start | bytes 30728 | tf_op jit(solution)/shard_map/ppermute | solution.py:68
  56.1 5.5 %collective-permute-start.10 = (f32[8,320]{1,0:T(8,128)S(1)}, f32[8,320]{1,0:T(8,128)S(1)}, u32[]{:S(2)}, u32[]{:S(2)}) collective-permute-start(f32[8,320]{1,0:T(8,128)S(1)} %add.12), channel_id=1, source_target_pairs={{0,24},{1,25},{2,26},{3,27},{4,28},{5,29},{6,30},{7,31},{8,16},{9,... | collective-permute-start | bytes 30728 | tf_op jit(solution)/shard_map/ppermute | solution.py:68
  57.5 4.1 %collective-permute-start.8 = (f32[8,320]{1,0:T(8,128)S(1)}, f32[8,320]{1,0:T(8,128)S(1)}, u32[]{:S(2)}, u32[]{:S(2)}) collective-permute-start(f32[8,320]{1,0:T(8,128)S(1)} %add.12), channel_id=1, source_target_pairs={{0,8},{1,9},{2,10},{3,11},{4,12},{5,13},{6,14},{7,15},{8,0},{9,1},... | collective-permute-start | bytes 30728 | tf_op jit(solution)/shard_map/ppermute | solution.py:68
  61.6 3.0 %collective-permute-start.11 = (f32[8,320]{1,0:T(8,128)S(1)}, f32[8,320]{1,0:T(8,128)S(1)}, u32[]{:S(2)}, u32[]{:S(2)}) collective-permute-start(f32[8,320]{1,0:T(8,128)S(1)} %add_add_fusion.refs_0_), channel_id=1, source_target_pairs={{0,2},{1,3},{2,0},{3,1},{4,6},{5,7},{6,4},{7,5},{8,10},{9,11},{10,... | collective-permute-start | bytes 30728 | tf_op jit(solution)/shard_map/ppermute | solution.py:68
  61.7 3.8 %collective-permute-start.12 = (f32[8,320]{1,0:T(8,128)S(1)}, f32[8,320]{1,0:T(8,128)S(1)}, u32[]{:S(2)}, u32[]{:S(2)}) collective-permute-start(f32[8,320]{1,0:T(8,128)S(1)} %add_add_fusion.refs_0_), channel_id=1, source_target_pairs={{0,4},{1,5},{2,6},{3,7},{4,0},{5,1},{6,2},{7,3},{8,12},{9,13},{10,... | collective-permute-start | bytes 30728 | tf_op jit(solution)/shard_map/ppermute | solution.py:68
  62.0 3.5 %collective-permute-start.13 = (f32[8,320]{1,0:T(8,128)S(1)}, f32[8,320]{1,0:T(8,128)S(1)}, u32[]{:S(2)}, u32[]{:S(2)}) collective-permute-start(f32[8,320]{1,0:T(8,128)S(1)} %add_add_fusion.refs_0_), channel_id=1, source_target_pairs={{0,6},{1,7},{2,4},{3,5},{4,2},{5,3},{6,0},{7,1},{8,14},{9,15},{10,... | collective-permute-start | bytes 30728 | tf_op jit(solution)/shard_map/ppermute | solution.py:68
